TPU v7x, 32 devices: a whole 2x2x4 slice. The times are simulated.
32 devices in a mesh: dp: 4 (over y, x), kv: 4 (over z), tp: 2 (over core).
Axes of the slice: x: 2, y: 2, z: 4, core: 2. Of those that a mesh axis runs over, the one named last changes fastest.
Arguments:
- resid: bfloat16 [16, 2048], P('dp', ('kv', 'tp')), may hold values from -45 to 45
- norm_gain: bfloat16 [3, 2048], P(None, ('kv', 'tp')), may hold values from 0.099609375 to 1.8984375
- ffn_gate: bfloat16 [2, 2048, 5632], P(None, None, ('kv', 'tp')), may hold values from -0.125 to 0.125
- ffn_up: bfloat16 [2, 2048, 5632], P(None, None, ('kv', 'tp')), may hold values from -0.125 to 0.125
- ffn_down: bfloat16 [2, 5632, 2048], P(None, ('kv', 'tp')), may hold values from -0.109375 to 0.109375
- w_x: bfloat16 [2048, 64, 64], P(None, 'kv', 'tp'), may hold values from -0.125 to 0.125
- w_z: bfloat16 [2048, 64, 64], P(None, 'kv', 'tp'), may hold values from -0.125 to 0.125
- w_bc: bfloat16 [2048, 2, 8, 128], P('kv'), may hold values from -0.125 to 0.125
- w_dt: bfloat16 [2048, 64], P('kv'), may hold values from -0.125 to 0.125
- dt_bias: float32 [64], replicated, may hold values from -2 to 0.5
- a_log: float32 [64], replicated, may hold values from -1.5 to 1.5
- d_skip: float32 [64], replicated, may hold values from 0.5 to 1.5
- conv_wx: bfloat16 [4, 64, 64], P(None, None, 'tp'), may hold values from -3 to 3
- conv_wbc: bfloat16 [4, 2, 8, 128], replicated, may hold values from -3 to 3
- conv_x: bfloat16 [16, 3, 64, 64], P(('dp', 'kv'), None, None, 'tp'), may hold values from -6 to 6
- conv_bc: bfloat16 [16, 3, 2, 8, 128], P(('dp', 'kv')), may hold values from -6 to 6
- ssm_state: float32 [16, 64, 64, 128], P(('dp', 'kv'), None, 'tp'), may hold values from -3 to 3
- w_out: bfloat16 [64, 64, 2048], P(None, 'tp', 'kv'), may hold values from -0.09375 to 0.09375
Outputs:
- final: bfloat16 [16, 2048], P('dp', ('kv', 'tp'))
All inputs are finite; a program needn't handle non-finite values.
Results may differ from a plain program's by a relative error of at most 0.018.
Values may be sent and summed in bfloat16 or wider, within the bound.
No kernel may reach another device: no remote copies, remote signals or barrier semaphores. Data moves between devices by JAX's collectives and lax.ppermute only.
A program may use at most 64 MiB of HBM per device.

v0:
```python
import jax
import jax.numpy as jnp
from jax import lax
from jax.sharding import PartitionSpec as P

D = 2048
EPS = 1e-06


def normalize(rows, gain):
    values = rows.astype(jnp.float32)
    scale = lax.rsqrt(jnp.mean(values * values, axis=1, keepdims=True) + EPS)
    return (values * scale * gain.astype(jnp.float32).reshape(1, -1)).astype(jnp.bfloat16)


def feed_forward(normed, w_gate, w_up, w_down):
    gate = jnp.dot(normed, w_gate, preferred_element_type=jnp.float32)
    upper = jnp.dot(normed, w_up, preferred_element_type=jnp.float32)
    hidden = (jax.nn.silu(gate) * upper).astype(jnp.bfloat16)
    return jnp.dot(hidden, w_down, preferred_element_type=jnp.float32)


def add_half(base, sums):
    return (base.astype(jnp.float32) + 0.5 * sums).astype(jnp.bfloat16)


def ffn_totals(partial_value):
    return lax.psum(partial_value, ("kv", "tp"))


def short_conv(history, newest, taps):
    window = jnp.concatenate(
        [history.astype(jnp.float32), newest.astype(jnp.float32)[:, None]], axis=1
    )
    return jax.nn.silu(jnp.sum(window * taps.astype(jnp.float32)[None], axis=1))


def state_step(
    xs_new,
    zeta,
    bc_new,
    dt_raw,
    conv_x,
    conv_bc,
    ssm_state,
    conv_wx,
    conv_wbc,
    dt_bias,
    a_log,
    d_skip,
):
    xconv = short_conv(conv_x, xs_new, conv_wx)
    bconv = short_conv(conv_bc, bc_new, conv_wbc)
    heads = xconv.shape[1]
    groups = bconv.shape[2]
    bmat = jnp.repeat(bconv[:, 0], heads // groups, axis=1)
    cmat = jnp.repeat(bconv[:, 1], heads // groups, axis=1)
    step_size = jax.nn.softplus(dt_raw + dt_bias[None, :])
    decay = jnp.exp(-step_size * jnp.exp(a_log)[None, :])
    updated = (
        decay[:, :, None, None] * ssm_state
        + (step_size[:, :, None] * xconv)[..., None] * bmat[:, :, None, :]
    )
    mixed = (
        jnp.einsum("shpn,shn->shp", updated, cmat, precision=lax.Precision.HIGHEST)
        + d_skip[None, :, None] * xconv
    )
    return (mixed * jax.nn.silu(zeta.astype(jnp.float32))).astype(jnp.bfloat16)


def group_terms(slab, w_bc, w_dt):
    span = slab.shape[1]
    flat_bc = w_bc.reshape(span, -1)
    bc_part = jnp.dot(slab, flat_bc, preferred_element_type=jnp.float32)
    dt_part = jnp.dot(slab, w_dt, preferred_element_type=jnp.float32)
    return (
        lax.psum_scatter(bc_part, "kv", scatter_dimension=0, tiled=True),
        lax.psum_scatter(dt_part, "kv", scatter_dimension=0, tiled=True),
    )


def mix_partial(
    normed,
    w_x,
    w_z,
    w_bc,
    w_dt,
    dt_bias,
    a_log,
    d_skip,
    conv_wx,
    conv_wbc,
    conv_x,
    conv_bc,
    ssm_state,
    w_out,
):
    rows = normed.shape[0]
    local_heads = w_x.shape[1]
    half = w_x.shape[2]
    xs_part = (
        jnp.dot(normed, w_x.reshape(D, -1), preferred_element_type=jnp.float32)
        .astype(jnp.bfloat16)
        .reshape(rows, local_heads, half)
    )
    zeta_part = (
        jnp.dot(normed, w_z.reshape(D, -1), preferred_element_type=jnp.float32)
        .astype(jnp.bfloat16)
        .reshape(rows, local_heads, half)
    )
    xs_new, zeta = (
        lax.all_to_all(xs_part, "kv", split_axis=0, concat_axis=1, tiled=True),
        lax.all_to_all(zeta_part, "kv", split_axis=0, concat_axis=1, tiled=True),
    )
    span = w_bc.shape[0]
    slab = lax.dynamic_slice_in_dim(normed, lax.axis_index("kv") * span, span, 1)
    bc_sum, dt_raw = group_terms(slab, w_bc, w_dt)
    bc_new = bc_sum.astype(jnp.bfloat16).reshape((bc_sum.shape[0],) + w_bc.shape[1:])
    mixed = state_step(
        xs_new,
        zeta,
        bc_new,
        dt_raw,
        conv_x,
        conv_bc,
        ssm_state,
        conv_wx,
        conv_wbc,
        dt_bias,
        a_log,
        d_skip,
    )
    flat_out = w_out.reshape(-1, w_out.shape[2])
    piece = lax.all_gather(mixed, "kv", axis=0, tiled=True)
    return jnp.dot(piece.reshape(piece.shape[0], -1), flat_out, preferred_element_type=jnp.float32)


def per_device(
    resid,
    norm_gain,
    ffn_gate,
    ffn_up,
    ffn_down,
    w_x,
    w_z,
    w_bc,
    w_dt,
    dt_bias,
    a_log,
    d_skip,
    conv_wx,
    conv_wbc,
    conv_x,
    conv_bc,
    ssm_state,
    w_out,
):
    mixer_args = (
        w_x,
        w_z,
        w_bc,
        w_dt,
        dt_bias,
        a_log,
        d_skip,
        conv_wx,
        conv_wbc,
        conv_x,
        conv_bc,
        ssm_state,
        w_out,
    )
    rows, gains = (
        lax.all_gather(resid, ("kv", "tp"), axis=1, tiled=True),
        lax.all_gather(norm_gain, ("kv", "tp"), axis=1, tiled=True),
    )
    first = add_half(
        rows,
        ffn_totals(feed_forward(normalize(rows, gains[0]), ffn_gate[0], ffn_up[0], ffn_down[0])),
    )
    partial_value = mix_partial(normalize(first, gains[1]), *mixer_args)
    span = partial_value.shape[1]
    block = lax.dynamic_slice_in_dim(first, lax.axis_index("kv") * span, span, 1)
    joined = (block.astype(jnp.float32) + lax.psum(partial_value, "tp")).astype(jnp.bfloat16)
    second = lax.all_gather(joined, "kv", axis=1, tiled=True)
    final = add_half(
        second,
        ffn_totals(feed_forward(normalize(second, gains[2]), ffn_gate[1], ffn_up[1], ffn_down[1])),
    )
    width = resid.shape[1]
    return lax.dynamic_slice_in_dim(final, lax.axis_index(("kv", "tp")) * width, width, 1)


def solution(mesh):
    placed = (
        P("dp", ("kv", "tp")),
        P(None, ("kv", "tp")),
        P(None, None, ("kv", "tp")),
        P(None, None, ("kv", "tp")),
        P(None, ("kv", "tp"), None),
        P(None, "kv", "tp"),
        P(None, "kv", "tp"),
        P("kv", None, None, None),
        P("kv", None),
        P(),
        P(),
        P(),
        P(None, None, "tp"),
        P(),
        P(("dp", "kv"), None, None, "tp"),
        P(("dp", "kv"), None, None, None, None),
        P(("dp", "kv"), None, "tp", None),
        P(None, "tp", "kv"),
    )
    return jax.shard_map(
        per_device, mesh=mesh, in_specs=placed, out_specs=P("dp", ("kv", "tp")), check_vma=False
    )
```

profile of v0, /device:TPU:0, one launch (start us, length us, event | category | flops | bytes accessed | tf_op | source)
XLA Modules:
  0.0 168.5 jit_solution(16530086735748407296)
XLA Ops:
  0.0 14.7 %all_gather.12 = bf16[4,2048]{1,0:T(4,128)(2,1)S(1)} all-gather(bf16[4,256]{1,0:T(4,128)(2,1)} %param.18), channel_id=1, replica_groups=mesh['dp'=4,'kv'=4,'tp'=2] {'kv','tp'}, dimensions={1}, use_global_device_ids=true | all-gather | bytes 18432 | tf_op jit(solution)/shard_map/all_gather | solution.py:174
  14.7 0.1 fusion.48
  14.9 12.9 %all_gather.13 = bf16[3,2048]{1,0:T(4,128)(2,1)S(1)} all-gather(bf16[3,256]{1,0:T(4,128)(2,1)} %param.19), channel_id=1, replica_groups=mesh['dp'=4,'kv'=4,'tp'=2] {'kv','tp'}, dimensions={1}, use_global_device_ids=true | all-gather | bytes 13824 | tf_op jit(solution)/shard_map/all_gather | solution.py:175
  27.8 2.7 %fusion.10 = f32[4,704]{1,0:T(4,128)S(1)} fusion(bf16[2,2048,704]{1,2,0:T(8,128)(2,1)} %param.20, bf16[4,2048]{1,0:T(4,128)(2,1)S(1)} %all_gather.12, f32[2048]{0:T(1024)S(1)} %bitcast.113, f32[4]{0:T(128)S(1)} %add_rsqrt_fusion.2), kind=kOutput, calls=%fused_computation.10 | convolution fusion | flops 11567104 | bytes 2919440 | tf_op jit(solution)/shard_map/dot_general | solution.py:17
  30.5 4.4 %fusion.6 = f32[4,2048]{1,0:T(4,128)S(1)} fusion(bf16[2,704,2048]{2,1,0:T(8,128)(2,1)} %param.22, bf16[2,2048,704]{1,2,0:T(8,128)(2,1)} %param.21, f32[4,704]{1,0:T(4,128)S(1)} %fusion.10, bf16[4,2048]{1,0:T(4,128)(2,1)S(1)} %all_gather.12, f32[2048]{0:T(1024)S(1)} %bitcast.114, f32[4]{0:T(128)S(1)} %add_rsqrt_fusion.2), kind=kOutput, calls=%fused_computation.6 | convolution fusion | flops 23118336 | bytes 5835792 | tf_op jit(solution)/shard_map/dot_general | solution.py:20
  34.8 26.7 %psum.21 = f32[4,2048]{1,0:T(4,128)S(1)} all-reduce(f32[4,2048]{1,0:T(4,128)S(1)} %fusion.6), channel_id=1, replica_groups=mesh['dp'=4,'kv'=4,'tp'=2] {'kv','tp'}, use_global_device_ids=true, to_apply=%region_1.2 | all-reduce | flops 8192 | bytes 65536 | tf_op jit(solution)/shard_map/psum | solution.py:28
  61.5 0.1 fusion.45
  61.8 0.6 convolution_convert_fusion.1
  62.5 0.7 reshape.219
  63.2 3.2 %all-to-all-start = ((bf16[4,2,256]{2,1,0:T(2,128)(2,1)}), bf16[4,2,256]{2,1,0:T(2,128)(2,1)S(1)}, u32[]{:S(2)}, u32[]{:S(2)}) async-start(bf16[4,2,256]{2,1,0:T(2,128)(2,1)} %reshape.219), calls=%async_computation | async-start | bytes 8192 | tf_op jit(solution)/shard_map/all_to_all | solution.py:112
  66.5 2.2 %convolution_convert_fusion = bf16[4,512]{1,0:T(4,128)(2,1)S(1)} fusion(bf16[4,2048]{1,0:T(4,128)(2,1)S(1)} %fusion.47, bf16[2048,512]{0,1:T(8,128)(2,1)} %bitcast.109), kind=kOutput, calls=%fused_computation.26 | convolution fusion | flops 8390656 | bytes 2117632 | tf_op jit(solution)/shard_map/dot_general | solution.py:107
  68.7 0.1 fusion.69
  68.9 2.0 %fusion.18 = f32[4,2048]{1,0:T(4,128)S(1)} fusion(bf16[64,8,16,128]{3,2,1,0:T(8,128)(2,1)} %bitcast.108, bf16[4,2048]{1,0:T(4,128)(2,1)S(1)} %fusion.47, s32[]{:T(128)S(6)} %select_n.11), kind=kOutput, calls=%fused_computation.18 | convolution fusion | flops 8388608 | bytes 2134020 | tf_op jit(solution)/shard_map/dot_general | solution.py:74
  70.9 0.6 dynamic-slice
  71.4 19.8 %all-reduce.2 = (bf16[4,2048]{1,0:T(4,128)(2,1)S(1)}, f32[4,64]{1,0:T(4,128)S(1)}) all-reduce(f32[4,2048]{1,0:T(4,128)S(1)} %fusion.18, f32[4,64]{1,0:T(4,128)S(1)} %fusion.69), channel_id=4, replica_groups=mesh['dp'=4,'kv'=4,'tp'=2] {'kv'}, use_global_device_ids=true, to_apply=%region_5.6.clone | all-reduce | flops 8448 | bytes 51200
  91.2 0.7 fusion.60
  92.1 0.7 reshape.217
  92.8 3.2 %all-to-all-start.1 = ((bf16[4,2,256]{2,1,0:T(2,128)(2,1)}), bf16[4,2,256]{2,1,0:T(2,128)(2,1)S(1)}, u32[]{:S(2)}, u32[]{:S(2)}) async-start(bf16[4,2,256]{2,1,0:T(2,128)(2,1)} %reshape.217), calls=%async_computation.1 | async-start | bytes 8192 | tf_op jit(solution)/shard_map/all_to_all | solution.py:113
  96.0 0.7 fusion.75
  96.7 0.1 reshape.220
  96.9 4.7 %all-to-all-done.1 = bf16[4,2,256]{2,1,0:T(2,128)(2,1)S(1)} async-done(((bf16[4,2,256]{2,1,0:T(2,128)(2,1)}), bf16[4,2,256]{2,1,0:T(2,128)(2,1)S(1)}, u32[]{:S(2)}, u32[]{:S(2)}) %all-to-all-start.1) | async-done | bytes 4128 | tf_op jit(solution)/shard_map/all_to_all | solution.py:113
  101.9 1.9 %fusion.33 = f32[64,1,32]{2,1,0:T(1,128)S(1)} fusion(f32[64,128,1]{1,2,0:T(1,128)S(1)} %bitcast.110, f32[1,64,32,128]{3,2,1,0:T(8,128)S(1)} %copy-done.1, f32[64,128]{1,0:T(8,128)S(1)} %broadcast_bitcast_fusion, f32[64,32]{1,0:T(8,128)S(1)} %copy.28, f32[64]{0:T(128)S(1)} %get-tuple-element.7), kind=kOutput, calls=%fused_computation.28 | convolution fusion | flops 3932160 | bytes 1130752 | tf_op jit(solution)/shard_map/shpn,shn->shp/dot_general | solution.py:65
  103.9 13.1 %all-gather.1 = bf16[4,64,32]{1,2,0:T(8,128)(2,1)S(1)} all-gather(bf16[1,64,32]{1,2,0:T(8,128)(2,1)S(1)} %fusion.64), channel_id=2, replica_groups=mesh['dp'=4,'kv'=4,'tp'=2] {'kv'}, dimensions={0}, use_global_device_ids=true | all-gather | bytes 20480 | tf_op jit(solution)/shard_map/all_gather | solution.py:134
  117.0 0.1 copy.35
  117.1 2.0 %convolution_bitcast_fusion = f32[4,512]{1,0:T(4,128)S(1)} fusion(bf16[4,64,32]{2,0,1:T(4,128)(2,1)S(1)} %copy.35, bf16[64,32,512]{2,1,0:T(8,128)(2,1)} %param.35), kind=kOutput, calls=%fused_computation.25 | convolution fusion | flops 8388608 | bytes 2121728 | tf_op jit(solution)/shard_map/dot_general | solution.py:135
  119.2 2.5 %psum.22 = f32[4,512]{1,0:T(4,128)S(1)} all-reduce(f32[4,512]{1,0:T(4,128)S(1)} %convolution_bitcast_fusion), channel_id=1, replica_groups=mesh['dp'=4,'kv'=4,'tp'=2] {'tp'}, use_global_device_ids=true, to_apply=%region_7.8 | all-reduce | flops 2048 | bytes 16384 | tf_op jit(solution)/shard_map/psum | solution.py:184
  121.6 13.2 %all_gather.15 = bf16[4,2048]{1,0:T(4,128)(2,1)S(1)} all-gather(bf16[4,512]{1,0:T(4,128)(2,1)S(1)} %add_convert_fusion), channel_id=1, replica_groups=mesh['dp'=4,'kv'=4,'tp'=2] {'kv'}, dimensions={1}, use_global_device_ids=true | all-gather | bytes 20480 | tf_op jit(solution)/shard_map/all_gather | solution.py:185
  134.8 0.1 multiply_reduce_fusion.1
  135.0 2.7 %fusion.4 = f32[4,704]{1,0:T(4,128)S(1)} fusion(bf16[2,2048,704]{1,2,0:T(8,128)(2,1)} %param.20, f32[2048]{0:T(1024)S(1)} %bitcast.111, f32[4]{0:T(128)S(1)} %add_rsqrt_fusion, bf16[4,2048]{1,0:T(4,128)(2,1)S(1)} %all_gather.15), kind=kOutput, calls=%fused_computation.4 | convolution fusion | flops 11567104 | bytes 2919440 | tf_op jit(solution)/shard_map/dot_general | solution.py:17
  137.7 4.4 %fusion = f32[4,2048]{1,0:T(4,128)S(1)} fusion(bf16[2,704,2048]{2,1,0:T(8,128)(2,1)} %param.22, bf16[2,2048,704]{1,2,0:T(8,128)(2,1)} %param.21, f32[4,704]{1,0:T(4,128)S(1)} %fusion.4, f32[2048]{0:T(1024)S(1)} %bitcast.112, f32[4]{0:T(128)S(1)} %add_rsqrt_fusion, bf16[4,2048]{1,0:T(4,128)(2,1)S(1)} %all_gather.15), kind=kOutput, calls=%fused_computation | convolution fusion | flops 23118336 | bytes 5835792 | tf_op jit(solution)/shard_map/dot_general | solution.py:20
  142.0 25.9 %psum.23 = f32[4,2048]{1,0:T(4,128)S(1)} all-reduce(f32[4,2048]{1,0:T(4,128)S(1)} %fusion), channel_id=1, replica_groups=mesh['dp'=4,'kv'=4,'tp'=2] {'kv','tp'}, use_global_device_ids=true, to_apply=%region_9.10 | all-reduce | flops 8192 | bytes 65536 | tf_op jit(solution)/shard_map/psum | solution.py:28
  168.0 0.6 fusion.67
  (46 shorter events, 0.9 us)
Async XLA Ops:
  0.0 61.7 %copy-start = (bf16[2048,16,32]{0,2,1:T(8,128)(2,1)S(1)}, bf16[2048,16,32]{0,2,1:T(8,128)(2,1)}, u32[]{:S(2)}) copy-start(bf16[2048,16,32]{0,2,1:T(8,128)(2,1)} %param.23) | copy-start | bytes 6291460
  34.8 33.9 %copy-start.2 = (bf16[512,64]{0,1:T(8,128)(2,1)S(1)}, bf16[512,64]{0,1:T(8,128)(2,1)}, u32[]{:S(2)}) copy-start(bf16[512,64]{0,1:T(8,128)(2,1)} %param.26) | copy-start | bytes 196612
  61.7 9.1 %copy-start.10 = (u32[32]{0:T(128)S(1)}, u32[32]{0:T(128)}, u32[]{:S(2)}) copy-start(u32[32]{0:T(128)} %constant.45) | copy-start | bytes 388
  61.7 30.2 %copy-start.5 = (bf16[4,2,8,128]{3,2,1,0:T(8,128)(2,1)S(1)}, bf16[4,2,8,128]{3,2,1,0:T(8,128)(2,1)}, u32[]{:S(2)}) copy-start(bf16[4,2,8,128]{3,2,1,0:T(8,128)(2,1)} %param.31) | copy-start | bytes 49156
  61.8 30.2 %copy-start.6 = (bf16[1,3,2,8,128]{4,3,2,1,0:T(8,128)(2,1)S(1)}, bf16[1,3,2,8,128]{4,3,2,1,0:T(8,128)(2,1)}, u32[]{:S(2)}) copy-start(bf16[1,3,2,8,128]{4,3,2,1,0:T(8,128)(2,1)} %param.33) | copy-start | bytes 36868
  61.8 34.2 %copy-start.8 = (f32[64]{0:T(128)S(1)}, f32[64]{0:T(128)}, u32[]{:S(2)}) copy-start(f32[64]{0:T(128)} %param.28) | copy-start | bytes 772
  61.8 34.2 %copy-start.9 = (f32[64]{0:T(128)S(1)}, f32[64]{0:T(128)}, u32[]{:S(2)}) copy-start(f32[64]{0:T(128)} %param.27) | copy-start | bytes 772
  62.4 39.3 %copy-start.3 = (bf16[4,64,32]{1,2,0:T(8,128)(2,1)S(1)}, bf16[4,64,32]{1,2,0:T(8,128)(2,1)}, u32[]{:S(2)}) copy-start(bf16[4,64,32]{1,2,0:T(8,128)(2,1)} %param.30) | copy-start | bytes 49156
  62.4 39.3 %copy-start.4 = (bf16[1,3,64,32]{2,3,1,0:T(8,128)(2,1)S(1)}, bf16[1,3,64,32]{2,3,1,0:T(8,128)(2,1)}, u32[]{:S(2)}) copy-start(bf16[1,3,64,32]{2,3,1,0:T(8,128)(2,1)} %param.32) | copy-start | bytes 36868
  62.4 39.4 %copy-start.1 = (f32[1,64,32,128]{3,2,1,0:T(8,128)S(1)}, f32[1,64,32,128]{3,2,1,0:T(8,128)}, u32[]{:S(2)}) copy-start(f32[1,64,32,128]{3,2,1,0:T(8,128)} %param.34) | copy-start | bytes 3145732
  63.2 29.5 %all-to-all-start = ((bf16[4,2,256]{2,1,0:T(2,128)(2,1)}), bf16[4,2,256]{2,1,0:T(2,128)(2,1)S(1)}, u32[]{:S(2)}, u32[]{:S(2)}) async-start(bf16[4,2,256]{2,1,0:T(2,128)(2,1)} %reshape.219), calls=%async_computation | async-start | bytes 8192 | tf_op jit(solution)/shard_map/all_to_all | solution.py:112
  66.5 37.4 %copy-start.7 = (f32[64]{0:T(128)S(1)}, f32[64]{0:T(128)}, u32[]{:S(2)}) copy-start(f32[64]{0:T(128)} %param.29) | copy-start | bytes 772
  92.8 8.8 %all-to-all-start.1 = ((bf16[4,2,256]{2,1,0:T(2,128)(2,1)}), bf16[4,2,256]{2,1,0:T(2,128)(2,1)S(1)}, u32[]{:S(2)}, u32[]{:S(2)}) async-start(bf16[4,2,256]{2,1,0:T(2,128)(2,1)} %reshape.217), calls=%async_computation.1 | async-start | bytes 8192 | tf_op jit(solution)/shard_map/all_to_all | solution.py:113
where the time goes:
time: 169 us
  blocking collectives  129 us (76%)
  matrix products  22.9 us (14%)
  starting transfers between devices  6.47 us (4%)
  waiting for transfers between devices  4.68 us (3%)
  local copies, waits for them, and re-layouts  3.47 us (2%)
  other arithmetic  1.89 us (1%)
    psum x2, blocking collectives, ffn_totals(): return lax.psum(partial_value, ('kv', 'tp'))  52.6 us
    unnamed x1, blocking collectives  19.8 us
    all_gather x1, blocking collectives, per_device(): lax.all_gather(resid, ('kv', 'tp'), axis=1, tiled=True)  14.7 us
    all_gather x1, blocking collectives, per_device(): second = lax.all_gather(joined, 'kv', axis=1, tiled=True)  13.2 us
    all_gather x1, blocking collectives, mix_partial(): piece = lax.all_gather(mixed, 'kv', axis=0, tiled=True)  13.1 us
    all_gather x1, blocking collectives, per_device(): lax.all_gather(norm_gain, ('kv', 'tp'), axis=1, tiled=True)  12.9 us
    dot_general x2, matrix products, feed_forward(): return jnp.dot(hidden, w_down, preferred_element_type=jnp.float32)  8.72 us
    dot_general x2, matrix products, feed_forward(): gate = jnp.dot(normed, w_gate, preferred_element_type=jnp.float32)  5.31 us
  transfers between devices with their start and end apart: 2, of which 1 were waited for; matrix products, arithmetic and copies ran while one was open for 4% of the time, Pallas kernels for 0%

commit v1 on v0

--- a/solution.py
+++ b/solution.py
@@ -25,7 +25,7 @@
 
 
 def ffn_totals(partial_value):
-    return lax.psum(partial_value, ("kv", "tp"))
+    return lax.psum(lax.psum(partial_value, "tp"), "kv")
 
 
 def short_conv(history, newest, taps):

time: 169 us -> 156 us (0.923)
  blocking collectives: 129 us -> 116 us
    psum x2 -> x4, blocking collectives: 52.6 us -> 39.8 us  [ffn_totals(): return lax.psum(lax.psum(partial_value, 'tp'), 'kv')]
  transfers between devices with their start and end apart: 2 -> 2, of which waited for: 1 -> 1; matrix products, arithmetic and copies ran while one was open for 4% -> 5% of each run, Pallas kernels for 0% -> 0%
where the time goes in v1:
time: 156 us
  blocking collectives  116 us (74%)
  matrix products  22.9 us (15%)
  starting transfers between devices  6.47 us (4%)
  waiting for transfers between devices  4.68 us (3%)
  local copies, waits for them, and re-layouts  3.47 us (2%)
  other arithmetic  1.9 us (1%)
    psum x4, blocking collectives, ffn_totals(): return lax.psum(lax.psum(partial_value, 'tp'), 'kv')  39.8 us
    unnamed x1, blocking collectives  19.8 us
    all_gather x1, blocking collectives, per_device(): lax.all_gather(resid, ('kv', 'tp'), axis=1, tiled=True)  14.7 us
    all_gather x1, blocking collectives, per_device(): second = lax.all_gather(joined, 'kv', axis=1, tiled=True)  13.2 us
    all_gather x1, blocking collectives, mix_partial(): piece = lax.all_gather(mixed, 'kv', axis=0, tiled=True)  13.1 us
    all_gather x1, blocking collectives, per_device(): lax.all_gather(norm_gain, ('kv', 'tp'), axis=1, tiled=True)  12.9 us
    dot_general x2, matrix products, feed_forward(): return jnp.dot(hidden, w_down, preferred_element_type=jnp.float32)  8.72 us
    dot_general x2, matrix products, feed_forward(): gate = jnp.dot(normed, w_gate, preferred_element_type=jnp.float32)  5.31 us
  transfers between devices with their start and end apart: 2, of which 1 were waited for; matrix products, arithmetic and copies ran while one was open for 5% of the time, Pallas kernels for 0%

profile of v1, /device:TPU:0, one launch (start us, length us, event | category | flops | bytes accessed | tf_op | source)
XLA Modules:
  0.0 155.9 jit_solution(8590855458713456822)
XLA Ops:
  0.0 14.7 %all_gather.12 = bf16[4,2048]{1,0:T(4,128)(2,1)S(1)} all-gather(bf16[4,256]{1,0:T(4,128)(2,1)} %param.18), channel_id=1, replica_groups=mesh['dp'=4,'kv'=4,'tp'=2] {'kv','tp'}, dimensions={1}, use_global_device_ids=true | all-gather | bytes 18432 | tf_op jit(solution)/shard_map/all_gather | solution.py:174
  14.7 0.1 fusion.48
  14.9 12.9 %all_gather.13 = bf16[3,2048]{1,0:T(4,128)(2,1)S(1)} all-gather(bf16[3,256]{1,0:T(4,128)(2,1)} %param.19), channel_id=1, replica_groups=mesh['dp'=4,'kv'=4,'tp'=2] {'kv','tp'}, dimensions={1}, use_global_device_ids=true | all-gather | bytes 13824 | tf_op jit(solution)/shard_map/all_gather | solution.py:175
  27.8 2.7 %fusion.10 = f32[4,704]{1,0:T(4,128)S(1)} fusion(bf16[2,2048,704]{1,2,0:T(8,128)(2,1)} %param.20, bf16[4,2048]{1,0:T(4,128)(2,1)S(1)} %all_gather.12, f32[2048]{0:T(1024)S(1)} %bitcast.113, f32[4]{0:T(128)S(1)} %add_rsqrt_fusion.2), kind=kOutput, calls=%fused_computation.10 | convolution fusion | flops 11567104 | bytes 2919440 | tf_op jit(solution)/shard_map/dot_general | solution.py:17
  30.5 4.4 %fusion.6 = f32[4,2048]{1,0:T(4,128)S(1)} fusion(bf16[2,704,2048]{2,1,0:T(8,128)(2,1)} %param.22, bf16[2,2048,704]{1,2,0:T(8,128)(2,1)} %param.21, f32[4,704]{1,0:T(4,128)S(1)} %fusion.10, bf16[4,2048]{1,0:T(4,128)(2,1)S(1)} %all_gather.12, f32[2048]{0:T(1024)S(1)} %bitcast.114, f32[4]{0:T(128)S(1)} %add_rsqrt_fusion.2), kind=kOutput, calls=%fused_computation.6 | convolution fusion | flops 23118336 | bytes 5835792 | tf_op jit(solution)/shard_map/dot_general | solution.py:20
  34.8 3.7 %psum.35 = f32[4,2048]{1,0:T(4,128)S(1)} all-reduce(f32[4,2048]{1,0:T(4,128)S(1)} %fusion.6), channel_id=1, replica_groups=mesh['dp'=4,'kv'=4,'tp'=2] {'tp'}, use_global_device_ids=true, to_apply=%region_1.2 | all-reduce | flops 8192 | bytes 65536 | tf_op jit(solution)/shard_map/psum | solution.py:28
  38.5 16.5 %psum.36 = f32[4,2048]{1,0:T(4,128)S(1)} all-reduce(f32[4,2048]{1,0:T(4,128)S(1)} %psum.35), channel_id=1, replica_groups=mesh['dp'=4,'kv'=4,'tp'=2] {'kv'}, use_global_device_ids=true, to_apply=%region_2.3 | all-reduce | flops 8192 | bytes 65536 | tf_op jit(solution)/shard_map/psum | solution.py:28
  55.0 0.1 fusion.45
  55.3 0.6 convolution_convert_fusion.1
  56.1 0.7 reshape.219
  56.7 3.2 %all-to-all-start = ((bf16[4,2,256]{2,1,0:T(2,128)(2,1)}), bf16[4,2,256]{2,1,0:T(2,128)(2,1)S(1)}, u32[]{:S(2)}, u32[]{:S(2)}) async-start(bf16[4,2,256]{2,1,0:T(2,128)(2,1)} %reshape.219), calls=%async_computation | async-start | bytes 8192 | tf_op jit(solution)/shard_map/all_to_all | solution.py:112
  60.0 2.2 %convolution_convert_fusion = bf16[4,512]{1,0:T(4,128)(2,1)S(1)} fusion(bf16[4,2048]{1,0:T(4,128)(2,1)S(1)} %fusion.47, bf16[2048,512]{0,1:T(8,128)(2,1)} %bitcast.109), kind=kOutput, calls=%fused_computation.26 | convolution fusion | flops 8390656 | bytes 2117632 | tf_op jit(solution)/shard_map/dot_general | solution.py:107
  62.2 0.1 fusion.69
  62.4 2.0 %fusion.18 = f32[4,2048]{1,0:T(4,128)S(1)} fusion(bf16[64,8,16,128]{3,2,1,0:T(8,128)(2,1)} %bitcast.108, bf16[4,2048]{1,0:T(4,128)(2,1)S(1)} %fusion.47, s32[]{:T(128)S(6)} %select_n.11), kind=kOutput, calls=%fused_computation.18 | convolution fusion | flops 8388608 | bytes 2134020 | tf_op jit(solution)/shard_map/dot_general | solution.py:74
  64.4 0.6 dynamic-slice
  65.0 19.8 %all-reduce.2 = (bf16[4,2048]{1,0:T(4,128)(2,1)S(1)}, f32[4,64]{1,0:T(4,128)S(1)}) all-reduce(f32[4,2048]{1,0:T(4,128)S(1)} %fusion.18, f32[4,64]{1,0:T(4,128)S(1)} %fusion.69), channel_id=4, replica_groups=mesh['dp'=4,'kv'=4,'tp'=2] {'kv'}, use_global_device_ids=true, to_apply=%region_6.7.clone | all-reduce | flops 8448 | bytes 51200
  84.8 0.7 fusion.60
  85.7 0.7 reshape.217
  86.3 3.2 %all-to-all-start.1 = ((bf16[4,2,256]{2,1,0:T(2,128)(2,1)}), bf16[4,2,256]{2,1,0:T(2,128)(2,1)S(1)}, u32[]{:S(2)}, u32[]{:S(2)}) async-start(bf16[4,2,256]{2,1,0:T(2,128)(2,1)} %reshape.217), calls=%async_computation.1 | async-start | bytes 8192 | tf_op jit(solution)/shard_map/all_to_all | solution.py:113
  89.6 0.7 fusion.75
  90.5 4.7 %all-to-all-done.1 = bf16[4,2,256]{2,1,0:T(2,128)(2,1)S(1)} async-done(((bf16[4,2,256]{2,1,0:T(2,128)(2,1)}), bf16[4,2,256]{2,1,0:T(2,128)(2,1)S(1)}, u32[]{:S(2)}, u32[]{:S(2)}) %all-to-all-start.1) | async-done | bytes 4128 | tf_op jit(solution)/shard_map/all_to_all | solution.py:113
  95.5 1.9 %fusion.33 = f32[64,1,32]{2,1,0:T(1,128)S(1)} fusion(f32[64,128,1]{1,2,0:T(1,128)S(1)} %bitcast.110, f32[1,64,32,128]{3,2,1,0:T(8,128)S(1)} %copy-done.1, f32[64,128]{1,0:T(8,128)S(1)} %broadcast_bitcast_fusion, f32[64,32]{1,0:T(8,128)S(1)} %copy.28, f32[64]{0:T(128)S(1)} %get-tuple-element.7), kind=kOutput, calls=%fused_computation.28 | convolution fusion | flops 3932160 | bytes 1130752 | tf_op jit(solution)/shard_map/shpn,shn->shp/dot_general | solution.py:65
  97.5 13.1 %all-gather.1 = bf16[4,64,32]{1,2,0:T(8,128)(2,1)S(1)} all-gather(bf16[1,64,32]{1,2,0:T(8,128)(2,1)S(1)} %fusion.64), channel_id=2, replica_groups=mesh['dp'=4,'kv'=4,'tp'=2] {'kv'}, dimensions={0}, use_global_device_ids=true | all-gather | bytes 20480 | tf_op jit(solution)/shard_map/all_gather | solution.py:134
  110.7 2.0 %convolution_bitcast_fusion = f32[4,512]{1,0:T(4,128)S(1)} fusion(bf16[4,64,32]{2,0,1:T(4,128)(2,1)S(1)} %copy.35, bf16[64,32,512]{2,1,0:T(8,128)(2,1)} %param.35), kind=kOutput, calls=%fused_computation.25 | convolution fusion | flops 8388608 | bytes 2121728 | tf_op jit(solution)/shard_map/dot_general | solution.py:135
  112.7 2.5 %psum.37 = f32[4,512]{1,0:T(4,128)S(1)} all-reduce(f32[4,512]{1,0:T(4,128)S(1)} %convolution_bitcast_fusion), channel_id=1, replica_groups=mesh['dp'=4,'kv'=4,'tp'=2] {'tp'}, use_global_device_ids=true, to_apply=%region_8.9 | all-reduce | flops 2048 | bytes 16384 | tf_op jit(solution)/shard_map/psum | solution.py:184
  115.2 13.2 %all_gather.15 = bf16[4,2048]{1,0:T(4,128)(2,1)S(1)} all-gather(bf16[4,512]{1,0:T(4,128)(2,1)S(1)} %add_convert_fusion), channel_id=1, replica_groups=mesh['dp'=4,'kv'=4,'tp'=2] {'kv'}, dimensions={1}, use_global_device_ids=true | all-gather | bytes 20480 | tf_op jit(solution)/shard_map/all_gather | solution.py:185
  128.4 0.1 multiply_reduce_fusion.1
  128.6 2.7 %fusion.4 = f32[4,704]{1,0:T(4,128)S(1)} fusion(bf16[2,2048,704]{1,2,0:T(8,128)(2,1)} %param.20, f32[2048]{0:T(1024)S(1)} %bitcast.111, f32[4]{0:T(128)S(1)} %add_rsqrt_fusion, bf16[4,2048]{1,0:T(4,128)(2,1)S(1)} %all_gather.15), kind=kOutput, calls=%fused_computation.4 | convolution fusion | flops 11567104 | bytes 2919440 | tf_op jit(solution)/shard_map/dot_general | solution.py:17
  131.2 4.4 %fusion = f32[4,2048]{1,0:T(4,128)S(1)} fusion(bf16[2,704,2048]{2,1,0:T(8,128)(2,1)} %param.22, bf16[2,2048,704]{1,2,0:T(8,128)(2,1)} %param.21, f32[4,704]{1,0:T(4,128)S(1)} %fusion.4, f32[2048]{0:T(1024)S(1)} %bitcast.112, f32[4]{0:T(128)S(1)} %add_rsqrt_fusion, bf16[4,2048]{1,0:T(4,128)(2,1)S(1)} %all_gather.15), kind=kOutput, calls=%fused_computation | convolution fusion | flops 23118336 | bytes 5835792 | tf_op jit(solution)/shard_map/dot_general | solution.py:20
  135.6 3.4 %psum.38 = f32[4,2048]{1,0:T(4,128)S(1)} all-reduce(f32[4,2048]{1,0:T(4,128)S(1)} %fusion), channel_id=1, replica_groups=mesh['dp'=4,'kv'=4,'tp'=2] {'tp'}, use_global_device_ids=true, to_apply=%region_10.11 | all-reduce | flops 8192 | bytes 65536 | tf_op jit(solution)/shard_map/psum | solution.py:28
  139.0 16.2 %psum.39 = f32[4,2048]{1,0:T(4,128)S(1)} all-reduce(f32[4,2048]{1,0:T(4,128)S(1)} %psum.38), channel_id=1, replica_groups=mesh['dp'=4,'kv'=4,'tp'=2] {'kv'}, use_global_device_ids=true, to_apply=%region_11.12 | all-reduce | flops 8192 | bytes 65536 | tf_op jit(solution)/shard_map/psum | solution.py:28
  155.3 0.6 fusion.67
  (48 shorter events, 1.1 us)
Async XLA Ops:
  0.0 55.2 %copy-start = (bf16[2048,16,32]{0,2,1:T(8,128)(2,1)S(1)}, bf16[2048,16,32]{0,2,1:T(8,128)(2,1)}, u32[]{:S(2)}) copy-start(bf16[2048,16,32]{0,2,1:T(8,128)(2,1)} %param.23) | copy-start | bytes 6291460
  34.8 27.4 %copy-start.2 = (bf16[512,64]{0,1:T(8,128)(2,1)S(1)}, bf16[512,64]{0,1:T(8,128)(2,1)}, u32[]{:S(2)}) copy-start(bf16[512,64]{0,1:T(8,128)(2,1)} %param.26) | copy-start | bytes 196612
  55.2 9.1 %copy-start.10 = (u32[32]{0:T(128)S(1)}, u32[32]{0:T(128)}, u32[]{:S(2)}) copy-start(u32[32]{0:T(128)} %constant.45) | copy-start | bytes 388
  55.3 30.2 %copy-start.5 = (bf16[4,2,8,128]{3,2,1,0:T(8,128)(2,1)S(1)}, bf16[4,2,8,128]{3,2,1,0:T(8,128)(2,1)}, u32[]{:S(2)}) copy-start(bf16[4,2,8,128]{3,2,1,0:T(8,128)(2,1)} %param.31) | copy-start | bytes 49156
  55.3 30.2 %copy-start.6 = (bf16[1,3,2,8,128]{4,3,2,1,0:T(8,128)(2,1)S(1)}, bf16[1,3,2,8,128]{4,3,2,1,0:T(8,128)(2,1)}, u32[]{:S(2)}) copy-start(bf16[1,3,2,8,128]{4,3,2,1,0:T(8,128)(2,1)} %param.33) | copy-start | bytes 36868
  55.3 34.3 %copy-start.8 = (f32[64]{0:T(128)S(1)}, f32[64]{0:T(128)}, u32[]{:S(2)}) copy-start(f32[64]{0:T(128)} %param.28) | copy-start | bytes 772
  55.3 34.3 %copy-start.9 = (f32[64]{0:T(128)S(1)}, f32[64]{0:T(128)}, u32[]{:S(2)}) copy-start(f32[64]{0:T(128)} %param.27) | copy-start | bytes 772
  55.9 39.4 %copy-start.3 = (bf16[4,64,32]{1,2,0:T(8,128)(2,1)S(1)}, bf16[4,64,32]{1,2,0:T(8,128)(2,1)}, u32[]{:S(2)}) copy-start(bf16[4,64,32]{1,2,0:T(8,128)(2,1)} %param.30) | copy-start | bytes 49156
  55.9 39.4 %copy-start.4 = (bf16[1,3,64,32]{2,3,1,0:T(8,128)(2,1)S(1)}, bf16[1,3,64,32]{2,3,1,0:T(8,128)(2,1)}, u32[]{:S(2)}) copy-start(bf16[1,3,64,32]{2,3,1,0:T(8,128)(2,1)} %param.32) | copy-start | bytes 36868
  56.0 39.5 %copy-start.1 = (f32[1,64,32,128]{3,2,1,0:T(8,128)S(1)}, f32[1,64,32,128]{3,2,1,0:T(8,128)}, u32[]{:S(2)}) copy-start(f32[1,64,32,128]{3,2,1,0:T(8,128)} %param.34) | copy-start | bytes 3145732
  56.7 29.6 %all-to-all-start = ((bf16[4,2,256]{2,1,0:T(2,128)(2,1)}), bf16[4,2,256]{2,1,0:T(2,128)(2,1)S(1)}, u32[]{:S(2)}, u32[]{:S(2)}) async-start(bf16[4,2,256]{2,1,0:T(2,128)(2,1)} %reshape.219), calls=%async_computation | async-start | bytes 8192 | tf_op jit(solution)/shard_map/all_to_all | solution.py:112
  60.0 37.4 %copy-start.7 = (f32[64]{0:T(128)S(1)}, f32[64]{0:T(128)}, u32[]{:S(2)}) copy-start(f32[64]{0:T(128)} %param.29) | copy-start | bytes 772
  86.3 8.8 %all-to-all-start.1 = ((bf16[4,2,256]{2,1,0:T(2,128)(2,1)}), bf16[4,2,256]{2,1,0:T(2,128)(2,1)S(1)}, u32[]{:S(2)}, u32[]{:S(2)}) async-start(bf16[4,2,256]{2,1,0:T(2,128)(2,1)} %reshape.217), calls=%async_computation.1 | async-start | bytes 8192 | tf_op jit(solution)/shard_map/all_to_all | solution.py:113
